TPU v7x, 128 devices: a whole 4x4x4 slice. The times are simulated.
128 devices in a mesh: fs: 32 (over z, y, core), tp: 4 (over x).
Axes of the slice: x: 4, y: 4, z: 4, core: 2. Of those that a mesh axis runs over, the one named last changes fastest.
Arguments:
- first_map: bfloat16 [24576, 2048], P('fs', 'tp'), may hold values from -6 to 6
- second_map: bfloat16 [24576, 2048], P('fs', 'tp'), may hold values from -6 to 6
- lambda_head: float32 [16], P('tp'), may hold values from 0.3 to 0.8
- head_gain: float32 [2048], P('tp'), may hold values from 0.1 to 1.9
- cot_output: bfloat16 [24576, 4096], P('fs'), may hold values from -6 to 6
- layer_input: bfloat16 [24576, 4096], P('fs'), may hold values from -6 to 6
- cot_values: bfloat16 [24576, 2048], P('fs', 'tp'), may hold values from -16 to 16
- factor_value: bfloat16 [4096, 256], P('fs'), may hold values from -1 to 1
- factor_output: bfloat16 [4096, 256], P('fs'), may hold values from -1 to 1
- weight_value: float32 [4096, 2048], P('fs', 'tp'), may hold values from -6 to 6
- weight_output: float32 [2048, 4096], P('tp', 'fs'), may hold values from -6 to 6
- first_value: float32 [256, 2048], P('fs', 'tp'), may hold values from -6 to 6
- second_value: float32 [256, 2048], P('fs', 'tp'), may hold values from 0.05 to 1
- first_output: float32 [256, 2048], P('fs', 'tp'), may hold values from -6 to 6
- second_output: float32 [256, 2048], P('fs', 'tp'), may hold values from 0.05 to 1
Outputs:
- new_weight_value: float32 [4096, 2048], P('fs', 'tp')
- new_first_value: float32 [256, 2048], P('fs', 'tp')
- new_second_value: float32 [256, 2048], P('fs', 'tp')
- copy_value: bfloat16 [4096, 2048], P(None, 'tp')
- new_weight_output: float32 [2048, 4096], P('tp', 'fs')
- new_first_output: float32 [256, 2048], P('fs', 'tp')
- new_second_output: float32 [256, 2048], P('fs', 'tp')
- copy_output: bfloat16 [2048, 4096], P('tp')
All inputs are finite; a program needn't handle non-finite values.
Results may differ from a plain program's by a relative error of at most 0.002.
Values may be sent and summed in bfloat16 or wider, within the bound.
A program may use at most 128 MiB of HBM per device.

v0:
```python
import math
import jax
import jax.numpy as jnp
from jax import lax
from jax.sharding import Mesh
from jax.sharding import PartitionSpec as P

RANK = 256
HV = 2048
FS = ("fs_0", "fs_1", "fs_2")
FS_TP = ("fs_0", "fs_1", "fs_2", "tp")
norm_epsilon = 1e-06
first_decay = 0.9
second_decay = 0.95
learn_rate = 0.1


def in_blocks(value, dim, devices):
    dims = value.shape
    tiles = value.reshape(*dims[:dim], devices, dims[dim] // devices, *dims[dim + 1 :])
    return jnp.moveaxis(tiles, dim, 0)


def sent_and_summed(value, axis, dim):
    devices = lax.axis_size(axis)
    tiles = lax.all_to_all(in_blocks(value, dim, devices), axis, 0, 0, tiled=True)
    return jnp.sum(tiles, axis=0)


def side_by_side(arrays, axis, dim, along):
    ends, at = ([], 0)
    for a in arrays[:-1]:
        at += a.shape[along]
        ends.append(at)
    both = jnp.concatenate(arrays, axis=along)
    return tuple(jnp.split(lax.all_gather(both, axis, axis=dim, tiled=True), ends, axis=along))


def over_axes(value, axes):
    for axis in axes:
        value = lax.psum(value, axis)
    return value


def gather_turned(arrays, axis, dims):
    turned = [jnp.moveaxis(a, dim, 0) for a, dim in zip(arrays, dims)]
    both = jnp.concatenate([t.reshape(len(t), -1) for t in turned], axis=1)
    result, at, outs = (lax.all_gather(both, axis, axis=0, tiled=True), 0, [])
    for t, dim in zip(turned, dims):
        slab = result[:, at : at + t[0].size].reshape(-1, *t.shape[1:])
        outs.append(jnp.moveaxis(slab, 0, dim))
        at += t[0].size
    return tuple(outs)


def head_output(first_map, second_map, lambda_head, head_gain):
    heads_here = lambda_head.shape[0]
    head_width = first_map.shape[1] // heads_here
    count_rows = first_map.shape[0]
    spread = jnp.repeat(lambda_head, head_width)
    differ = first_map.astype(jnp.float32) - spread[None, :] * second_map.astype(jnp.float32)
    grouped = differ.reshape(count_rows, heads_here, head_width)
    scaled = grouped * lax.rsqrt(jnp.mean(grouped * grouped, -1, keepdims=True) + norm_epsilon)
    return (scaled.reshape(count_rows, heads_here * head_width) * head_gain[None, :]).astype(
        jnp.bfloat16
    )


def moments(projected, clip_factor, first_old, second_old):
    scaled = clip_factor * projected
    first_new = first_decay * first_old + (1.0 - first_decay) * scaled
    second_new = second_decay * second_old + (1.0 - second_decay) * scaled * scaled
    return (first_new, second_new, first_new * lax.rsqrt(second_new))


def low_rank(left, right):
    return sent_and_summed(
        lax.dot_general(
            left,
            right,
            (((0,), (0,)), ((), ())),
            precision=lax.Precision.HIGHEST,
            preferred_element_type=jnp.float32,
        ),
        FS,
        0,
    )


def shards(
    first_map,
    second_map,
    lambda_head,
    head_gain,
    cot_output,
    layer_input,
    cot_values,
    factor_value,
    factor_output,
    weight_value,
    weight_output,
    first_value,
    second_value,
    first_output,
    second_output,
):
    heads_out = head_output(first_map, second_map, lambda_head, head_gain)
    factor_v32 = factor_value.astype(jnp.float32)
    factor_o32 = factor_output.astype(jnp.float32)
    whole_value, whole_output = side_by_side((factor_value, factor_output), FS, 0, 1)
    mapped_value = jnp.dot(layer_input, whole_value, preferred_element_type=jnp.float32)
    mapped_output = jnp.dot(cot_output, whole_output, preferred_element_type=jnp.float32)
    low_value = low_rank(mapped_value, cot_values.astype(jnp.float32))
    low_output = low_rank(mapped_output, heads_out.astype(jnp.float32))
    partial_value = jnp.sum(low_value * low_value) + jnp.sum(low_output * low_output)
    total = over_axes(partial_value, FS_TP)
    clip_factor = jnp.minimum(1.0, math.sqrt(RANK * HV) * lax.rsqrt(total + norm_epsilon))
    first_v, second_v, ratio_value = moments(low_value, clip_factor, first_value, second_value)
    first_o, second_o, ratio_output = moments(low_output, clip_factor, first_output, second_output)
    pieces = side_by_side((ratio_value, ratio_output), FS, 0, 1)
    added_value = jnp.dot(
        factor_v32, pieces[0], precision=lax.Precision.HIGHEST, preferred_element_type=jnp.float32
    )
    added_output = lax.dot_general(
        pieces[1],
        factor_o32,
        (((0,), (1,)), ((), ())),
        precision=lax.Precision.HIGHEST,
        preferred_element_type=jnp.float32,
    )
    new_value = weight_value - learn_rate * added_value
    new_output = weight_output - learn_rate * added_output
    copy_value, copy_output = gather_turned(
        (new_value.astype(jnp.bfloat16), new_output.astype(jnp.bfloat16)), FS, (0, 1)
    )
    return (new_value, first_v, second_v, copy_value, new_output, first_o, second_o, copy_output)


def solution(mesh):
    torus = Mesh(mesh.devices.reshape(4, 4, 2, mesh.shape["tp"]), ("fs_0", "fs_1", "fs_2", "tp"))
    placed = (
        P(FS, "tp"),
        P(FS, "tp"),
        P("tp"),
        P("tp"),
        P(FS, None),
        P(FS, None),
        P(FS, "tp"),
        P(FS, None),
        P(FS, None),
        P(FS, "tp"),
        P("tp", FS),
        P(FS, "tp"),
        P(FS, "tp"),
        P(FS, "tp"),
        P(FS, "tp"),
    )
    return jax.shard_map(
        shards,
        mesh=torus,
        in_specs=placed,
        out_specs=(
            P(FS, "tp"),
            P(FS, "tp"),
            P(FS, "tp"),
            P(None, "tp"),
            P("tp", FS),
            P(FS, "tp"),
            P(FS, "tp"),
            P("tp", None),
        ),
        check_vma=False,
    )
```

profile of v0, /device:TPU:1, one launch (start us, length us, event | category | flops | bytes accessed | tf_op | source)
XLA Modules:
  0.0 256.5 jit_solution(15353092697436282198)
XLA Ops:
  7.2 1.6 pad_maximum_fusion.1
  8.9 0.7 broadcast_bitcast_fusion
  9.6 2.8 %fusion.6 = f32[768,512]{1,0:T(8,128)} fusion(bf16[768,512]{1,0:T(8,128)(2,1)} %param.16, bf16[768,512]{1,0:T(8,128)(2,1)} %param.15, f32[512]{0:T(512)S(1)} %broadcast_bitcast_fusion), kind=kLoop, calls=%fused_computation.9 | loop fusion | flops 1966080 | bytes 3147776 | tf_op jit(solution)/shard_map/mul | solution.py:63
  12.4 1.8 mul.106
  14.1 0.9 reduce_sum.47
  15.1 45.5 %all-gather.4.cloned.1.call-done = bf16[4096,512]{1,0:T(8,128)(2,1)} async-done(((bf16[128,512]{1,0:T(8,128)(2,1)}), bf16[4096,512]{1,0:T(8,128)(2,1)}) %all-gather.4.cloned.1.call-update) | async-done | bytes 4194320 | tf_op jit(solution)/shard_map/all_gather | solution.py:36
  60.6 5.3 %fusion.2 = f32[256,768]{1,0:T(8,128)S(1)} fusion(bf16[768,4096]{1,0:T(8,128)(2,1)} %param.20, bf16[4096,512]{1,0:T(8,128)(2,1)} %all-gather.4.cloned.1.call-done), kind=kOutput, calls=%fused_computation.3 | convolution fusion | flops 1610612736 | bytes 9175040 | tf_op jit(solution)/shard_map/dot_general | solution.py:111
  65.9 1.6 convolution_bitcast_fusion
  67.5 5.3 %all-to-all-start = ((f32[32,8,512]{2,1,0:T(8,128)}), f32[32,8,512]{2,1,0:T(8,128)S(1)}, u32[]{:S(2)}, u32[]{:S(2)}) async-start(f32[32,8,512]{2,1,0:T(8,128)} %convolution_bitcast_fusion), calls=%async_computation | async-start | bytes 1048576 | tf_op jit(solution)/shard_map/all_to_all | solution.py:26
  72.8 5.3 %fusion.7 = f32[32,8,768]{2,1,0:T(8,128)S(1)} fusion(bf16[768,4096]{1,0:T(8,128)(2,1)} %param.19, bf16[4096,512]{1,0:T(8,128)(2,1)} %all-gather.4.cloned.1.call-done), kind=kOutput, calls=%fused_computation.10 | convolution fusion | flops 1610612736 | bytes 9175040 | tf_op jit(solution)/shard_map/dot_general | solution.py:112
  78.1 1.0 mul.107
  79.2 0.2 copy-done.2
  79.5 1.8 fusion.14
  81.4 2.9 %all-to-all-done = f32[32,8,512]{2,1,0:T(8,128)S(1)} async-done(((f32[32,8,512]{2,1,0:T(8,128)}), f32[32,8,512]{2,1,0:T(8,128)S(1)}, u32[]{:S(2)}, u32[]{:S(2)}) %all-to-all-start) | async-done | bytes 524320 | tf_op jit(solution)/shard_map/all_to_all | solution.py:26
  84.2 4.6 %all-to-all-start.1 = ((f32[32,8,512]{2,1,0:T(8,128)}), f32[32,8,512]{2,1,0:T(8,128)S(1)}, u32[]{:S(2)}, u32[]{:S(2)}) async-start(f32[32,8,512]{2,1,0:T(8,128)} %fusion.14), calls=%async_computation.1 | async-start | bytes 1048576 | tf_op jit(solution)/shard_map/all_to_all | solution.py:26
  89.0 0.6 multiply_reduce_fusion.1
  89.6 10.7 %all-to-all-done.1 = f32[32,8,512]{2,1,0:T(8,128)S(1)} async-done(((f32[32,8,512]{2,1,0:T(8,128)}), f32[32,8,512]{2,1,0:T(8,128)S(1)}, u32[]{:S(2)}, u32[]{:S(2)}) %all-to-all-start.1) | async-done | bytes 524320 | tf_op jit(solution)/shard_map/all_to_all | solution.py:26
  100.4 0.6 multiply_reduce_fusion
  102.3 7.4 %psum.28 = f32[]{:T(128)} all-reduce(f32[]{:T(128)S(6)} %add.39), channel_id=1, replica_groups=mesh['fs_0'=4,'fs_1'=4,'fs_2'=2,'tp'=4] {'fs_0'}, use_global_device_ids=true, to_apply=%region_5.0 | all-reduce | flops 1 | bytes 8 | tf_op jit(solution)/shard_map/psum | solution.py:41
  109.6 8.4 %psum.29 = f32[]{:T(128)} all-reduce(f32[]{:T(128)} %psum.28), channel_id=1, replica_groups=mesh['fs_0'=4,'fs_1'=4,'fs_2'=2,'tp'=4] {'fs_1'}, use_global_device_ids=true, to_apply=%region_6.0 | all-reduce | flops 1 | bytes 8 | tf_op jit(solution)/shard_map/psum | solution.py:41
  118.1 5.8 %psum.30 = f32[]{:T(128)} all-reduce(f32[]{:T(128)} %psum.29), channel_id=1, replica_groups=mesh['fs_0'=4,'fs_1'=4,'fs_2'=2,'tp'=4] {'fs_2'}, use_global_device_ids=true, to_apply=%region_7.0 | all-reduce | flops 1 | bytes 8 | tf_op jit(solution)/shard_map/psum | solution.py:41
  123.9 9.0 %psum.31 = f32[]{:T(128)} all-reduce(f32[]{:T(128)} %psum.30), channel_id=1, replica_groups=mesh['fs_0'=4,'fs_1'=4,'fs_2'=2,'tp'=4] {'tp'}, use_global_device_ids=true, to_apply=%region_8.0 | all-reduce | flops 1 | bytes 8 | tf_op jit(solution)/shard_map/psum | solution.py:41
  133.6 0.6 rsqrt_multiply_fusion
  134.3 0.6 pad_maximum_fusion.2
  135.1 39.8 %all-gather.6.cloned.1.call-done = f32[256,1024]{1,0:T(8,128)} async-done(((f32[8,1024]{1,0:T(8,128)}), f32[256,1024]{1,0:T(8,128)}) %all-gather.6.cloned.1.call-update) | async-done | bytes 1048592 | tf_op jit(solution)/shard_map/all_gather | solution.py:36
  175.0 1.7 fusion.10
  176.7 1.7 fusion.24
  178.4 0.7 pad_maximum_fusion
  179.1 0.8 copy.33
  180.0 57.5 %all-gather.8.cloned.1.call-done = bf16[4096,1024]{0,1:T(8,128)(2,1)} async-done(((bf16[128,1024]{0,1:T(8,128)(2,1)}), bf16[4096,1024]{0,1:T(8,128)(2,1)}) %all-gather.8.cloned.1.call-update) | async-done | bytes 8388624 | tf_op jit(solution)/shard_map/all_gather | solution.py:48
  237.5 6.0 %slice_bitcast_fusion = (bf16[512,4096]{1,0:T(8,128)(2,1)}, bf16[4096,512]{0,1:T(8,128)(2,1)}) fusion(bf16[4096,1024]{0,1:T(8,128)(2,1)} %all-gather.8.cloned.1.call-done), kind=kLoop, calls=%fused_computation | loop fusion | bytes 16777216 | tf_op jit(solution)/shard_map/transpose | solution.py:51
  243.5 6.4 %copy.34 = bf16[4096,512]{1,0:T(8,128)(2,1)} copy(bf16[4096,512]{0,1:T(8,128)(2,1)} %get-tuple-element.39) | data formatting | bytes 8388608
  (36 shorter events, 0.7 us)
Async XLA Ops:
  7.2 58.7 %copy-start = (bf16[768,512]{1,0:T(8,128)(2,1)S(1)}, bf16[768,512]{1,0:T(8,128)(2,1)}, u32[]{:S(2)}) copy-start(bf16[768,512]{1,0:T(8,128)(2,1)} %param.21) | copy-start | bytes 2359300
  7.2 53.5 %all-gather.4.cloned.1.call-start = ((), (), s32[]{:S(2)}) async-start(), calls=%async_computation.2 | async-start | bytes 4325376 | tf_op jit(solution)/shard_map/all_gather | solution.py:36
  67.5 16.7 %all-to-all-start = ((f32[32,8,512]{2,1,0:T(8,128)}), f32[32,8,512]{2,1,0:T(8,128)S(1)}, u32[]{:S(2)}, u32[]{:S(2)}) async-start(f32[32,8,512]{2,1,0:T(8,128)} %convolution_bitcast_fusion), calls=%async_computation | async-start | bytes 1048576 | tf_op jit(solution)/shard_map/all_to_all | solution.py:26
  72.8 6.3 %copy-start.12 = (f32[512]{0:T(512)S(1)}, f32[512]{0:T(512)}, u32[]{:S(2)}) copy-start(f32[512]{0:T(512)} %param.18) | copy-start | bytes 6148
  78.1 1.1 copy-start.1
  78.1 1.4 copy-start.2
  81.3 52.3 %copy-start.8 = (f32[8,512]{1,0:T(8,128)S(1)}, f32[8,512]{1,0:T(8,128)}, u32[]{:S(2)}) copy-start(f32[8,512]{1,0:T(8,128)} %param.29) | copy-start | bytes 49156
  81.3 52.3 %copy-start.9 = (f32[8,512]{1,0:T(8,128)S(1)}, f32[8,512]{1,0:T(8,128)}, u32[]{:S(2)}) copy-start(f32[8,512]{1,0:T(8,128)} %param.28) | copy-start | bytes 49156
  81.3 52.3 %copy-start.10 = (f32[8,512]{1,0:T(8,128)S(1)}, f32[8,512]{1,0:T(8,128)}, u32[]{:S(2)}) copy-start(f32[8,512]{1,0:T(8,128)} %param.27) | copy-start | bytes 49156
  81.3 52.3 %copy-start.11 = (f32[8,512]{1,0:T(8,128)S(1)}, f32[8,512]{1,0:T(8,128)}, u32[]{:S(2)}) copy-start(f32[8,512]{1,0:T(8,128)} %param.26) | copy-start | bytes 49156
  81.3 53.7 %copy-start.5 = (f32[128,512]{1,0:T(8,128)S(1)}, f32[128,512]{1,0:T(8,128)}, u32[]{:S(2)}) copy-start(f32[128,512]{1,0:T(8,128)} %param.24) | copy-start | bytes 786436
  81.3 93.6 %copy-start.4 = (f32[512,128]{1,0:T(8,128)S(1)}, f32[512,128]{1,0:T(8,128)}, u32[]{:S(2)}) copy-start(f32[512,128]{1,0:T(8,128)} %param.25) | copy-start | bytes 786436
  81.3 93.6 %copy-start.6 = (bf16[128,256]{1,0:T(8,128)(2,1)S(1)}, bf16[128,256]{1,0:T(8,128)(2,1)}, u32[]{:S(2)}) copy-start(bf16[128,256]{1,0:T(8,128)(2,1)} %param.23) | copy-start | bytes 196612
  81.3 95.3 %copy-start.7 = (bf16[128,256]{1,0:T(8,128)(2,1)S(1)}, bf16[128,256]{1,0:T(8,128)(2,1)}, u32[]{:S(2)}) copy-start(bf16[128,256]{1,0:T(8,128)(2,1)} %param.22) | copy-start | bytes 196612
  84.2 16.1 %all-to-all-start.1 = ((f32[32,8,512]{2,1,0:T(8,128)}), f32[32,8,512]{2,1,0:T(8,128)S(1)}, u32[]{:S(2)}, u32[]{:S(2)}) async-start(f32[32,8,512]{2,1,0:T(8,128)} %fusion.14), calls=%async_computation.1 | async-start | bytes 1048576 | tf_op jit(solution)/shard_map/all_to_all | solution.py:26
  88.9 86.1 %all-gather.6.cloned.1.call-start = ((), (), s32[]{:S(2)}) async-start(), calls=%async_computation.3 | async-start | bytes 1081344 | tf_op jit(solution)/shard_map/all_gather | solution.py:36
  134.9 102.6 %all-gather.8.cloned.1.call-start = ((), (), s32[]{:S(2)}) async-start(), calls=%async_computation.4 | async-start | bytes 8650752 | tf_op jit(solution)/shard_map/all_gather | solution.py:48
  176.6 66.9 %copy-start.3 = (f32[512,128]{1,0:T(8,128)}, f32[512,128]{1,0:T(8,128)S(1)}, u32[]{:S(2)}) copy-start(f32[512,128]{1,0:T(8,128)S(1)} %fusion.10) | copy-start | bytes 786436
Sparse Core Ops, SparseCore 0:
  10.8 49.7 all-gather.3
  135.0 39.8 all-gather.5
  179.2 58.2 all-gather.7
where the time goes:
time: 257 us; the launch traced here: 256 us
  waiting for transfers between devices  157 us (61%)
  blocking collectives  30.6 us (12%)
  local copies, waits for them, and re-layouts  17.3 us (7%)
  matrix products  17.3 us (7%)
  between operations  16 us (6%)
  starting transfers between devices  10.1 us (4%)
  other arithmetic  8.61 us (3%)
    all_gather x2, waiting for transfers between devices, side_by_side(): lax.all_gather(both, axis, axis=dim, tiled=True)  85.4 us
    all_gather x1, waiting for transfers between devices, gather_turned(): result, at, outs = (lax.all_gather(both, axis, axis=0, tiled=True), 0, [])  57.5 us
    psum x4, blocking collectives, over_axes(): value = lax.psum(value, axis)  30.6 us
    all_to_all x2, waiting for transfers between devices, sent_and_summed(): lax.all_to_all(in_blocks(value, dim, devices), axis, 0, 0, tiled=True)  13.6 us
    all_to_all x2, starting transfers between devices, sent_and_summed(): lax.all_to_all(in_blocks(value, dim, devices), axis, 0, 0, tiled=True)  9.94 us
    unnamed x29, local copies, waits for them, and re-layouts  7.8 us
    transpose x1, local copies, waits for them, and re-layouts, gather_turned(): outs.append(jnp.moveaxis(slab, 0, dim))  6.03 us
    dot_general x1, matrix products, shards(): jnp.dot(cot_output, whole_output, preferred_element_type=jnp.float32)  5.27 us
  transfers between devices with their start and end apart: 5, of which 5 were waited for; matrix products, arithmetic and copies ran while one was open for 6% of the time, Pallas kernels for 0%

commit v1 on v0

--- a/solution.py
+++ b/solution.py
@@ -45,7 +45,13 @@
 def gather_turned(arrays, axis, dims):
     turned = [jnp.moveaxis(a, dim, 0) for a, dim in zip(arrays, dims)]
     both = jnp.concatenate([t.reshape(len(t), -1) for t in turned], axis=1)
-    result, at, outs = (lax.all_gather(both, axis, axis=0, tiled=True), 0, [])
+    result, at, outs = (
+        jnp.concatenate(
+            lax.all_to_all(jnp.stack([both] * lax.axis_size(axis)), axis, 0, 0), axis=0
+        ),
+        0,
+        [],
+    )
     for t, dim in zip(turned, dims):
         slab = result[:, at : at + t[0].size].reshape(-1, *t.shape[1:])
         outs.append(jnp.moveaxis(slab, 0, dim))

time: 257 us -> 326 us (1.27); the launches traced: 256 us -> 321 us
  waiting for transfers between devices: 157 us -> 199 us
  local copies, waits for them, and re-layouts: 17.3 us -> 34.2 us
  starting transfers between devices: 10.1 us -> 15.4 us
    all_to_all x0 -> x1, waiting for transfers between devices: none -> 99.9 us  [gather_turned(): lax.all_to_all(jnp.stack([both] * lax.axis_size(axis)), axis, 0, 0)]
    all_gather x1 -> x0, waiting for transfers between devices: 57.5 us -> none  [gather_turned(): result, at, outs = (lax.all_gather(both, axis, axis=0, tiled=True), 0, [])]
    all_to_all x0 -> x1, local copies, waits for them, and re-layouts: none -> 11.9 us  [gather_turned(): lax.all_to_all(jnp.stack([both] * lax.axis_size(axis)), axis, 0, 0)]
    all_to_all x0 -> x1, starting transfers between devices: none -> 5.35 us  [gather_turned(): lax.all_to_all(jnp.stack([both] * lax.axis_size(axis)), axis, 0, 0)]
    another operation x0 -> x1, local copies, waits for them, and re-layouts: none -> 5.11 us  [gather_turned(): jnp.stack([both] * lax.axis_size(axis))]
    unnamed x29 -> x31, local copies, waits for them, and re-layouts: 7.8 us -> 7.8 us
  transfers between devices with their start and end apart: 5 -> 5, of which waited for: 5 -> 5; matrix products, arithmetic and copies ran while one was open for 6% -> 5% of each run, Pallas kernels for 0% -> 0%
where the time goes in v1:
time: 326 us; the launch traced here: 321 us
  waiting for transfers between devices  199 us (61%)
  local copies, waits for them, and re-layouts  34.2 us (10%)
  blocking collectives  30.6 us (9%)
  matrix products  17.3 us (5%)
  between operations  16.3 us (5%)
  starting transfers between devices  15.4 us (5%)
  other arithmetic  7.91 us (2%)
    all_to_all x1, waiting for transfers between devices, gather_turned(): lax.all_to_all(jnp.stack([both] * lax.axis_size(axis)), axis, 0, 0)  99.9 us
    all_gather x2, waiting for transfers between devices, side_by_side(): lax.all_gather(both, axis, axis=dim, tiled=True)  85.4 us
    psum x4, blocking collectives, over_axes(): value = lax.psum(value, axis)  30.6 us
    all_to_all x2, waiting for transfers between devices, sent_and_summed(): lax.all_to_all(in_blocks(value, dim, devices), axis, 0, 0, tiled=True)  13.6 us
    all_to_all x1, local copies, waits for them, and re-layouts, gather_turned(): lax.all_to_all(jnp.stack([both] * lax.axis_size(axis)), axis, 0, 0)  11.9 us
    all_to_all x2, starting transfers between devices, sent_and_summed(): lax.all_to_all(in_blocks(value, dim, devices), axis, 0, 0, tiled=True)  9.94 us
    unnamed x31, local copies, waits for them, and re-layouts  7.8 us
  transfers between devices with their start and end apart: 5, of which 5 were waited for; matrix products, arithmetic and copies ran while one was open for 5% of the time, Pallas kernels for 0%

profile of v1, /device:TPU:1, one launch (start us, length us, event | category | flops | bytes accessed | tf_op | source)
XLA Modules:
  0.0 320.6 jit_solution(10125278360068570692)
XLA Ops:
  7.2 1.6 pad_maximum_fusion.1
  8.9 0.7 broadcast_bitcast_fusion
  9.6 2.8 fusion.6
  12.4 1.8 mul.106
  14.2 0.9 reduce_sum.47
  15.1 45.5 %all-gather.3.cloned.1.call-done = bf16[4096,512]{1,0:T(8,128)(2,1)} async-done(((bf16[128,512]{1,0:T(8,128)(2,1)}), bf16[4096,512]{1,0:T(8,128)(2,1)}) %all-gather.3.cloned.1.call-update) | async-done | bytes 4194320 | tf_op jit(solution)/shard_map/all_gather | solution.py:36
  60.6 5.3 %fusion.2 = f32[256,768]{1,0:T(8,128)S(1)} fusion(bf16[768,4096]{1,0:T(8,128)(2,1)} %param.20, bf16[4096,512]{1,0:T(8,128)(2,1)} %all-gather.3.cloned.1.call-done), kind=kOutput, calls=%fused_computation.3 | convolution fusion | flops 1610612736 | bytes 9175040 | tf_op jit(solution)/shard_map/dot_general | solution.py:117
  65.9 1.6 convolution_bitcast_fusion
  67.5 5.3 %all-to-all-start = ((f32[32,8,512]{2,1,0:T(8,128)}), f32[32,8,512]{2,1,0:T(8,128)S(1)}, u32[]{:S(2)}, u32[]{:S(2)}) async-start(f32[32,8,512]{2,1,0:T(8,128)} %convolution_bitcast_fusion), calls=%async_computation | async-start | bytes 1048576 | tf_op jit(solution)/shard_map/all_to_all | solution.py:26
  72.8 5.3 %fusion.7 = f32[32,8,768]{2,1,0:T(8,128)S(1)} fusion(bf16[768,4096]{1,0:T(8,128)(2,1)} %param.19, bf16[4096,512]{1,0:T(8,128)(2,1)} %all-gather.3.cloned.1.call-done), kind=kOutput, calls=%fused_computation.10 | convolution fusion | flops 1610612736 | bytes 9175040 | tf_op jit(solution)/shard_map/dot_general | solution.py:118
  78.1 1.0 mul.107
  79.5 1.8 fusion.14
  81.4 2.9 all-to-all-done
  84.2 4.6 %all-to-all-start.1 = ((f32[32,8,512]{2,1,0:T(8,128)}), f32[32,8,512]{2,1,0:T(8,128)S(1)}, u32[]{:S(2)}, u32[]{:S(2)}) async-start(f32[32,8,512]{2,1,0:T(8,128)} %fusion.14), calls=%async_computation.1 | async-start | bytes 1048576 | tf_op jit(solution)/shard_map/all_to_all | solution.py:26
  89.6 10.7 %all-to-all-done.1 = f32[32,8,512]{2,1,0:T(8,128)S(1)} async-done(((f32[32,8,512]{2,1,0:T(8,128)}), f32[32,8,512]{2,1,0:T(8,128)S(1)}, u32[]{:S(2)}, u32[]{:S(2)}) %all-to-all-start.1) | async-done | bytes 524320 | tf_op jit(solution)/shard_map/all_to_all | solution.py:26
  100.4 0.6 multiply_reduce_fusion
  102.3 7.4 %psum.28 = f32[]{:T(128)} all-reduce(f32[]{:T(128)S(6)} %add.39), channel_id=1, replica_groups=mesh['fs_0'=4,'fs_1'=4,'fs_2'=2,'tp'=4] {'fs_0'}, use_global_device_ids=true, to_apply=%region_5.0 | all-reduce | flops 1 | bytes 8 | tf_op jit(solution)/shard_map/psum | solution.py:41
  109.6 8.4 %psum.29 = f32[]{:T(128)} all-reduce(f32[]{:T(128)} %psum.28), channel_id=1, replica_groups=mesh['fs_0'=4,'fs_1'=4,'fs_2'=2,'tp'=4] {'fs_1'}, use_global_device_ids=true, to_apply=%region_6.0 | all-reduce | flops 1 | bytes 8 | tf_op jit(solution)/shard_map/psum | solution.py:41
  118.1 5.8 %psum.30 = f32[]{:T(128)} all-reduce(f32[]{:T(128)} %psum.29), channel_id=1, replica_groups=mesh['fs_0'=4,'fs_1'=4,'fs_2'=2,'tp'=4] {'fs_2'}, use_global_device_ids=true, to_apply=%region_7.0 | all-reduce | flops 1 | bytes 8 | tf_op jit(solution)/shard_map/psum | solution.py:41
  123.9 9.0 %psum.31 = f32[]{:T(128)} all-reduce(f32[]{:T(128)} %psum.30), channel_id=1, replica_groups=mesh['fs_0'=4,'fs_1'=4,'fs_2'=2,'tp'=4] {'tp'}, use_global_device_ids=true, to_apply=%region_8.0 | all-reduce | flops 1 | bytes 8 | tf_op jit(solution)/shard_map/psum | solution.py:41
  133.6 0.6 rsqrt_multiply_fusion
  134.3 0.6 pad_maximum_fusion.2
  135.1 39.9 %all-gather.5.cloned.1.call-done = f32[256,1024]{1,0:T(8,128)} async-done(((f32[8,1024]{1,0:T(8,128)}), f32[256,1024]{1,0:T(8,128)}) %all-gather.5.cloned.1.call-update) | async-done | bytes 1048592 | tf_op jit(solution)/shard_map/all_gather | solution.py:36
  175.0 1.7 fusion.10
  176.7 1.7 fusion.24
  178.4 5.1 %stack.2 = bf16[32,128,1024]{1,2,0:T(8,128)(2,1)} broadcast(bf16[128,1024]{0,1:T(8,128)(2,1)S(1)} %pad_maximum_fusion), dimensions={1,2} | broadcast | bytes 8650752 | tf_op jit(solution)/shard_map/stack | solution.py:50
  183.5 5.3 %all-to-all-start.2 = ((bf16[32,128,1024]{1,2,0:T(8,128)(2,1)}), bf16[32,128,1024]{1,2,0:T(8,128)(2,1)}, u32[]{:S(2)}, u32[]{:S(2)}) async-start(bf16[32,128,1024]{1,2,0:T(8,128)(2,1)} %stack.2), calls=%async_computation.2 | async-start | bytes 16777216 | tf_op jit(solution)/shard_map/all_to_all | solution.py:50
  188.9 0.8 copy.42
  189.7 99.9 %all-to-all-done.2 = bf16[32,128,1024]{1,2,0:T(8,128)(2,1)} async-done(((bf16[32,128,1024]{1,2,0:T(8,128)(2,1)}), bf16[32,128,1024]{1,2,0:T(8,128)(2,1)}, u32[]{:S(2)}, u32[]{:S(2)}) %all-to-all-start.2) | async-done | bytes 8388640 | tf_op jit(solution)/shard_map/all_to_all | solution.py:50
  289.6 11.9 %copy.41 = bf16[32,128,1024]{2,1,0:T(8,128)(2,1)} copy(bf16[32,128,1024]{1,2,0:T(8,128)(2,1)} %all-to-all-done.2) | data formatting | bytes 16777216 | tf_op jit(solution)/shard_map/all_to_all | solution.py:50
  301.5 5.8 %slice_bitcast_fusion = (bf16[512,4096]{0,1:T(8,128)(2,1)}, bf16[4096,512]{1,0:T(8,128)(2,1)}) fusion(bf16[4096,1024]{1,0:T(8,128)(2,1)} %bitcast.35), kind=kLoop, calls=%fused_computation | loop fusion | bytes 16777216 | tf_op jit(solution)/shard_map/transpose | solution.py:57
  307.4 6.4 %copy.43 = bf16[512,4096]{1,0:T(8,128)(2,1)} copy(bf16[512,4096]{0,1:T(8,128)(2,1)} %get-tuple-element.54) | data formatting | bytes 8388608
  (39 shorter events, 1.5 us)
Async XLA Ops:
  7.2 58.8 %copy-start = (bf16[768,512]{1,0:T(8,128)(2,1)S(1)}, bf16[768,512]{1,0:T(8,128)(2,1)}, u32[]{:S(2)}) copy-start(bf16[768,512]{1,0:T(8,128)(2,1)} %param.21) | copy-start | bytes 2359300
  7.2 53.5 %all-gather.3.cloned.1.call-start = ((), (), s32[]{:S(2)}) async-start(), calls=%async_computation.3 | async-start | bytes 4325376 | tf_op jit(solution)/shard_map/all_gather | solution.py:36
  67.5 16.7 %all-to-all-start = ((f32[32,8,512]{2,1,0:T(8,128)}), f32[32,8,512]{2,1,0:T(8,128)S(1)}, u32[]{:S(2)}, u32[]{:S(2)}) async-start(f32[32,8,512]{2,1,0:T(8,128)} %convolution_bitcast_fusion), calls=%async_computation | async-start | bytes 1048576 | tf_op jit(solution)/shard_map/all_to_all | solution.py:26
  72.8 6.3 %copy-start.13 = (f32[512]{0:T(512)S(1)}, f32[512]{0:T(512)}, u32[]{:S(2)}) copy-start(f32[512]{0:T(512)} %param.18) | copy-start | bytes 6148
  78.1 1.1 copy-start.2
  78.1 1.4 copy-start.3
  81.3 52.3 %copy-start.9 = (f32[8,512]{1,0:T(8,128)S(1)}, f32[8,512]{1,0:T(8,128)}, u32[]{:S(2)}) copy-start(f32[8,512]{1,0:T(8,128)} %param.29) | copy-start | bytes 49156
  81.3 52.3 %copy-start.10 = (f32[8,512]{1,0:T(8,128)S(1)}, f32[8,512]{1,0:T(8,128)}, u32[]{:S(2)}) copy-start(f32[8,512]{1,0:T(8,128)} %param.28) | copy-start | bytes 49156
  81.3 52.3 %copy-start.11 = (f32[8,512]{1,0:T(8,128)S(1)}, f32[8,512]{1,0:T(8,128)}, u32[]{:S(2)}) copy-start(f32[8,512]{1,0:T(8,128)} %param.27) | copy-start | bytes 49156
  81.3 52.3 %copy-start.12 = (f32[8,512]{1,0:T(8,128)S(1)}, f32[8,512]{1,0:T(8,128)}, u32[]{:S(2)}) copy-start(f32[8,512]{1,0:T(8,128)} %param.26) | copy-start | bytes 49156
  81.3 53.6 %copy-start.6 = (f32[128,512]{1,0:T(8,128)S(1)}, f32[128,512]{1,0:T(8,128)}, u32[]{:S(2)}) copy-start(f32[128,512]{1,0:T(8,128)} %param.24) | copy-start | bytes 786436
  81.3 93.6 %copy-start.5 = (f32[512,128]{1,0:T(8,128)S(1)}, f32[512,128]{1,0:T(8,128)}, u32[]{:S(2)}) copy-start(f32[512,128]{1,0:T(8,128)} %param.25) | copy-start | bytes 786436
  81.3 93.6 %copy-start.7 = (bf16[128,256]{1,0:T(8,128)(2,1)S(1)}, bf16[128,256]{1,0:T(8,128)(2,1)}, u32[]{:S(2)}) copy-start(bf16[128,256]{1,0:T(8,128)(2,1)} %param.23) | copy-start | bytes 196612
  81.3 95.3 %copy-start.8 = (bf16[128,256]{1,0:T(8,128)(2,1)S(1)}, bf16[128,256]{1,0:T(8,128)(2,1)}, u32[]{:S(2)}) copy-start(bf16[128,256]{1,0:T(8,128)(2,1)} %param.22) | copy-start | bytes 196612
  84.2 16.1 %all-to-all-start.1 = ((f32[32,8,512]{2,1,0:T(8,128)}), f32[32,8,512]{2,1,0:T(8,128)S(1)}, u32[]{:S(2)}, u32[]{:S(2)}) async-start(f32[32,8,512]{2,1,0:T(8,128)} %fusion.14), calls=%async_computation.1 | async-start | bytes 1048576 | tf_op jit(solution)/shard_map/all_to_all | solution.py:26
  88.9 86.1 %all-gather.5.cloned.1.call-start = ((), (), s32[]{:S(2)}) async-start(), calls=%async_computation.4 | async-start | bytes 1081344 | tf_op jit(solution)/shard_map/all_gather | solution.py:36
  176.6 6.9 %copy-start.4 = (f32[512,128]{1,0:T(8,128)}, f32[512,128]{1,0:T(8,128)S(1)}, u32[]{:S(2)}) copy-start(f32[512,128]{1,0:T(8,128)S(1)} %fusion.10) | copy-start | bytes 786436
  183.5 106.1 %all-to-all-start.2 = ((bf16[32,128,1024]{1,2,0:T(8,128)(2,1)}), bf16[32,128,1024]{1,2,0:T(8,128)(2,1)}, u32[]{:S(2)}, u32[]{:S(2)}) async-start(bf16[32,128,1024]{1,2,0:T(8,128)(2,1)} %stack.2), calls=%async_computation.2 | async-start | bytes 16777216 | tf_op jit(solution)/shard_map/all_to_all | solution.py:50
  307.4 6.4 %copy-start.1 = (bf16[768,512]{1,0:T(8,128)(2,1)S(1)}, bf16[768,512]{1,0:T(8,128)(2,1)}, u32[]{:S(2)}) copy-start(bf16[768,512]{1,0:T(8,128)(2,1)} %param.21) | copy-start | bytes 2359300
Sparse Core Ops, SparseCore 0:
  10.8 49.7 all-gather.2
  135.0 39.8 all-gather.4
